TPU v7x, 32 devices: a whole 2x2x4 slice. The times are simulated.
32 devices in a mesh: dp: 4 (over y, x), kv: 4 (over z), tp: 2 (over core).
Axes of the slice: x: 2, y: 2, z: 4, core: 2. Of those that a mesh axis runs over, the one named last changes fastest.
Arguments:
- tokens: bfloat16 [4, 3072, 2048], P('dp', 'kv'), may hold values from -60 to 60
- query_weight: bfloat16 [2048, 1024], P(None, 'tp'), may hold values from -0.125 to 0.125
- key_weight: bfloat16 [2048, 256], P(None, 'tp'), may hold values from -0.125 to 0.125
- value_weight: bfloat16 [2048, 256], P(None, 'tp'), may hold values from -0.125 to 0.125
- out_weight: bfloat16 [1024, 2048], P('tp'), may hold values from -3 to 3
- norm_gain: float32 [2048], P('tp'), may hold values from 0.1 to 1.9
- chosen_owner: int32 [4, 24, 4], P('dp'), may hold values from -1 to 3, as said below
- chosen_part: int32 [4, 24, 4], P('dp'), may hold values from 0 to 11, as said below
Outputs:
- attended: bfloat16 [4, 3072, 2048], P('dp', 'kv', 'tp')
Inputs may be any that keep to these rules, and one draw needn't show every extreme that they name: `chosen_owner`: within a row the indices other than -1 are different. Every named key block lies wholly before its query block's first position. Among the 6 rows of one index of kv, no index is named by more than 6 rows. `chosen_part`: 0 where the owner is -1.
All inputs are finite; a program needn't handle non-finite values.
Results may differ from a plain program's by a relative error of at most 0.014.
The roundings to bfloat16 on the way count: a program that leaves them out, or rounds other values in their place, can miss the bound.
Values may be sent and summed in bfloat16 or wider, within the bound.
A program may use at most 128 MiB of HBM per device.

v0:
```python
import jax
import jax.numpy as jnp
from jax import lax
from jax.sharding import PartitionSpec as P

D = 2048
HEAD_DIM = 64
QUERY_BLOCK = 128
KEY_BLOCK = 64
rope_base = 10000.0
norm_eps = 1e-06


def rotate(head_rows, positions):
    half_dim = head_rows.shape[-1] // 2
    frequency = rope_base ** (-jnp.arange(half_dim, dtype=jnp.float32) / half_dim)
    angles = positions.astype(jnp.float32)[:, None] * frequency
    cosine = jnp.cos(angles)[:, None, :]
    sine_part = jnp.sin(angles)[:, None, :]
    first_half = head_rows[..., :half_dim]
    second_half = head_rows[..., half_dim:]
    return jnp.concatenate(
        [
            first_half * cosine - second_half * sine_part,
            second_half * cosine + first_half * sine_part,
        ],
        axis=-1,
    )


def rank_within(flat_ids):
    entry_count = flat_ids.shape[0]
    same_owner = flat_ids[:, None] == flat_ids[None, :]
    earlier = jnp.arange(entry_count)[None, :] < jnp.arange(entry_count)[:, None]
    return jnp.sum(jnp.logical_and(same_owner, earlier), axis=1)


def body(
    tokens, query_weight, key_weight, value_weight, out_weight, norm_gain, chosen_owner, chosen_part
):
    row_data = tokens[0]
    tok_count = row_data.shape[0]
    devices = lax.axis_size("kv")
    my_index = lax.axis_index("kv")
    positions = my_index * tok_count + jnp.arange(tok_count, dtype=jnp.int32)
    heads_here = query_weight.shape[1] // HEAD_DIM
    kv_here = key_weight.shape[1] // HEAD_DIM
    group_size = heads_here // kv_here
    kv_width = kv_here * HEAD_DIM
    queries = rotate(
        jnp.dot(row_data, query_weight, preferred_element_type=jnp.float32).reshape(
            tok_count, heads_here, HEAD_DIM
        ),
        positions,
    ).astype(jnp.bfloat16)
    key_rows = (
        rotate(
            jnp.dot(row_data, key_weight, preferred_element_type=jnp.float32).reshape(
                tok_count, kv_here, HEAD_DIM
            ),
            positions,
        )
        .astype(jnp.bfloat16)
        .reshape(tok_count, kv_width)
    )
    value_rows = jnp.dot(row_data, value_weight, preferred_element_type=jnp.float32).astype(
        jnp.bfloat16
    )
    per_device = tok_count // KEY_BLOCK
    qblocks = tok_count // QUERY_BLOCK
    chosen_count = chosen_owner.shape[2]
    owner_ids = chosen_owner[0]
    part_ids = chosen_part[0]
    mine_owner = lax.dynamic_slice_in_dim(owner_ids, my_index * qblocks, qblocks, 0).reshape(
        qblocks * chosen_count
    )
    mine_valid = mine_owner >= 0
    key_blocks = key_rows.reshape(per_device, KEY_BLOCK, kv_width)
    value_blocks = value_rows.reshape(per_device, KEY_BLOCK, kv_width)
    every_owner = owner_ids.reshape(devices, qblocks * chosen_count)
    every_part = part_ids.reshape(devices, qblocks * chosen_count)
    every_rank = jax.vmap(rank_within)(every_owner)
    slot_ids = jnp.arange(qblocks, dtype=jnp.int32)
    picked_mask = jnp.logical_and(
        (every_owner == my_index)[:, None, :], every_rank[:, None, :] == slot_ids[None, :, None]
    )
    wanted = jnp.sum(jnp.where(picked_mask, every_part[:, None, :], 0), axis=2)
    send_keys = key_blocks[wanted]
    send_values = value_blocks[wanted]
    got_keys, got_values = (
        lax.all_to_all(send_keys, "kv", split_axis=0, concat_axis=0, tiled=True),
        lax.all_to_all(send_values, "kv", split_axis=0, concat_axis=0, tiled=True),
    )
    slot_index = jnp.where(mine_valid, mine_owner * qblocks + rank_within(mine_owner), 0)
    picked_keys = got_keys.reshape(devices * qblocks, KEY_BLOCK, kv_width)[slot_index]
    picked_values = got_values.reshape(devices * qblocks, KEY_BLOCK, kv_width)[slot_index]
    block_queries = queries.reshape(qblocks, QUERY_BLOCK, kv_here, group_size, HEAD_DIM)
    chosen_keys = picked_keys.reshape(qblocks, chosen_count * KEY_BLOCK, kv_here, HEAD_DIM)
    chosen_values = picked_values.reshape(qblocks, chosen_count * KEY_BLOCK, kv_here, HEAD_DIM)
    all_keys = jnp.concatenate(
        [chosen_keys, key_rows.reshape(qblocks, QUERY_BLOCK, kv_here, HEAD_DIM)], axis=1
    )
    all_values = jnp.concatenate(
        [chosen_values, value_rows.reshape(qblocks, QUERY_BLOCK, kv_here, HEAD_DIM)], axis=1
    )
    key_valid = jnp.broadcast_to(
        mine_valid.reshape(qblocks, chosen_count, 1), (qblocks, chosen_count, KEY_BLOCK)
    ).reshape(qblocks, chosen_count * KEY_BLOCK)
    far_mask = jnp.broadcast_to(
        key_valid[:, None, :], (qblocks, QUERY_BLOCK, chosen_count * KEY_BLOCK)
    )
    lower_mask = jnp.broadcast_to(
        (jnp.arange(QUERY_BLOCK)[:, None] >= jnp.arange(QUERY_BLOCK)[None, :])[None],
        (qblocks, QUERY_BLOCK, QUERY_BLOCK),
    )
    full_mask = jnp.concatenate([far_mask, lower_mask], axis=2)
    scores = jnp.einsum(
        "bqngd,bknd->bngqk", block_queries, all_keys, preferred_element_type=jnp.float32
    ) * HEAD_DIM ** (-0.5)
    scores = jnp.where(full_mask[:, None, None], scores, -jnp.inf)
    row_max = jnp.max(scores, axis=-1, keepdims=True)
    weights = jnp.exp(scores - row_max)
    weights = (weights / jnp.sum(weights, axis=-1, keepdims=True)).astype(jnp.bfloat16)
    mixed_rows = (
        jnp.einsum("bngqk,bknd->bqngd", weights, all_values, preferred_element_type=jnp.float32)
        .astype(jnp.bfloat16)
        .reshape(tok_count, heads_here * HEAD_DIM)
    )
    terms = jnp.dot(mixed_rows, out_weight, preferred_element_type=jnp.float32)
    projected = lax.psum_scatter(
        terms.astype(jnp.bfloat16), "tp", scatter_dimension=1, tiled=True
    ).astype(jnp.float32)
    row_total = lax.psum(jnp.sum(projected * projected, axis=1), "tp")
    scale_rows = lax.rsqrt(row_total / D + norm_eps)
    result = (projected * scale_rows[:, None] * norm_gain[None, :]).astype(jnp.bfloat16)
    return result[None]


def solution(mesh):
    placed = (
        P("dp", "kv", None),
        P(None, "tp"),
        P(None, "tp"),
        P(None, "tp"),
        P("tp", None),
        P("tp"),
        P("dp", None, None),
        P("dp", None, None),
    )
    return jax.shard_map(
        body, mesh=mesh, in_specs=placed, out_specs=P("dp", "kv", "tp"), check_vma=False
    )
```

profile of v0, /device:TPU:0, one launch (start us, length us, event | category | flops | bytes accessed | tf_op | source)
XLA Modules:
  0.0 117.1 jit_solution(5359210719336470150)
XLA Ops:
  6.5 0.6 iota_compare_fusion.2
  7.2 2.3 %copy.52 = bf16[2048,128]{0,1:T(8,128)(2,1)} copy(bf16[2048,128]{1,0:T(8,128)(2,1)} %param.10) | data formatting | bytes 1048576 | tf_op args[2]
  9.5 0.4 multiply_cosine_fusion
  9.9 2.2 %fusion.13 = f32[768,2,64]{0,2,1:T(8,128)S(1)} fusion(bf16[2,64,2048]{2,1,0:T(8,128)(2,1)} %bitcast.97, bf16[1,768,2048]{2,1,0:T(8,128)(2,1)S(1)} %copy-done), kind=kOutput, calls=%fused_computation.22 | convolution fusion | flops 402653184 | bytes 4063232 | tf_op jit(solution)/shard_map/dot_general | solution.py:58
  12.3 0.6 copy-done.2
  12.9 1.1 copy.53
  14.0 1.2 %convert_element_type.47 = bf16[12,64,128]{2,1,0:T(8,128)(2,1)S(1)} reshape(bf16[768,2,64]{2,1,0:T(2,128)(2,1)} %copy.53) | data formatting | bytes 393216 | tf_op jit(solution)/shard_map/convert_element_type | solution.py:63
  15.4 0.5 broadcast_compare_fusion.1
  15.9 1.5 %convert_reduce_fusion = s32[4,24]{1,0:T(4,128)} fusion(s32[4,24]{1,0:T(4,128)S(1)} %reshape_squeeze.3, pred[24,24]{1,0:T(8,128)(4,1)} %iota_compare_fusion.2), kind=kLoop, calls=%fused_computation.49 | loop fusion | flops 9120 | bytes 1344 | tf_op jit(solution)/shard_map/vmap()/reduce_sum | solution.py:35
  17.4 0.8 copy.43
  18.3 0.9 select_reduce_fusion
  19.3 1.4 %gather_fusion.2 = bf16[24,64,128]{2,1,0:T(8,128)(2,1)} fusion(bf16[12,64,128]{2,1,0:T(8,128)(2,1)S(1)} %convert_element_type.47, s32[1024]{0:T(1024)S(1)} %pad_clamp_fusion.1), kind=kCustom, calls=%fused_computation.2 | custom fusion | bytes 786528 | tf_op jit(solution)/shard_map/gather | solution.py:88
  20.7 6.3 %all-to-all-start.1 = ((bf16[4,6,64,128]{3,2,1,0:T(8,128)(2,1)}), bf16[4,6,64,128]{3,2,1,0:T(8,128)(2,1)}, u32[]{:S(2)}, u32[]{:S(2)}) async-start(bf16[4,6,64,128]{3,2,1,0:T(8,128)(2,1)} %bitcast.95), calls=%async_computation.1 | async-start | bytes 786432 | tf_op jit(solution)/shard_map/all_to_all | solution.py:91
  27.0 0.8 broadcast_multiply_fusion
  28.1 0.7 ge.38
  28.9 4.0 %copy.57 = bf16[2048,512]{0,1:T(8,128)(2,1)} copy(bf16[2048,512]{1,0:T(8,128)(2,1)} %param.9) | data formatting | bytes 4194304 | tf_op args[1]
  32.9 4.6 %fusion.11 = f32[768,8,64]{0,2,1:T(8,128)} fusion(bf16[8,64,2048]{2,1,0:T(8,128)(2,1)} %bitcast.92, bf16[1,768,2048]{2,1,0:T(8,128)(2,1)S(1)} %copy-done), kind=kOutput, calls=%fused_computation.20 | convolution fusion | flops 1610612736 | bytes 6815744 | tf_op jit(solution)/shard_map/dot_general | solution.py:51
  37.5 1.0 fusion.20
  38.5 1.3 %gather_fusion = bf16[24,64,128]{2,1,0:T(8,128)(2,1)} fusion(bf16[12,64,128]{2,1,0:T(8,128)(2,1)S(1)} %bitcast.93, s32[1024]{0:T(1024)S(1)} %pad_clamp_fusion.1), kind=kCustom, calls=%fused_computation | custom fusion | bytes 786528 | tf_op jit(solution)/shard_map/gather | solution.py:89
  39.8 0.2 convert_reduce_fusion.1
  40.0 0.5 fusion.43
  40.6 2.5 %subtract_convert_fusion = (bf16[768,8,32]{0,2,1:T(8,128)(2,1)}, bf16[768,8,32]{0,2,1:T(8,128)(2,1)}) fusion(f32[768,8,64]{0,2,1:T(8,128)} %fusion.11, f32[768,32]{0,1:T(8,128)S(1)} %get-tuple-element.12, f32[768,32]{0,1:T(8,128)S(1)} %get-tuple-element.11), kind=kLoop, calls=%fused_computation.35 | loop fusion | flops 1572864 | bytes 2555904 | tf_op jit(solution)/shard_map/convert.3
  43.0 5.1 %all-to-all-start = ((bf16[4,6,64,128]{3,2,1,0:T(8,128)(2,1)}), bf16[4,6,64,128]{3,2,1,0:T(8,128)(2,1)}, u32[]{:S(2)}, u32[]{:S(2)}) async-start(bf16[4,6,64,128]{3,2,1,0:T(8,128)(2,1)} %bitcast.94), calls=%async_computation | async-start | bytes 786432 | tf_op jit(solution)/shard_map/all_to_all | solution.py:92
  48.1 0.7 fusion.29
  48.8 0.9 reshape.247
  49.7 0.1 copy.51
  50.0 2.2 %concatenate.37 = bf16[6,128,2,4,32]{1,0,4,3,2:T(8,128)(2,1)} reshape(bf16[768,8,32]{0,2,1:T(8,128)(2,1)} %get-tuple-element.7) | data formatting | bytes 786432 | tf_op jit(solution)/shard_map/concatenate | solution.py:22
  52.2 1.9 %copy.58 = bf16[6,128,2,4,32]{1,4,3,2,0:T(8,128)(2,1)} copy(bf16[6,128,2,4,32]{1,0,4,3,2:T(8,128)(2,1)} %concatenate.37) | data formatting | bytes 786432 | tf_op jit(solution)/shard_map/concatenate | solution.py:22
  54.1 2.2 %concatenate.38 = bf16[6,128,2,4,32]{1,0,4,3,2:T(8,128)(2,1)} reshape(bf16[768,8,32]{0,2,1:T(8,128)(2,1)} %get-tuple-element.8) | data formatting | bytes 786432 | tf_op jit(solution)/shard_map/concatenate | solution.py:22
  56.3 1.9 %copy.59 = bf16[6,128,2,4,32]{1,4,3,2,0:T(8,128)(2,1)} copy(bf16[6,128,2,4,32]{1,0,4,3,2:T(8,128)(2,1)} %concatenate.38) | data formatting | bytes 786432 | tf_op jit(solution)/shard_map/concatenate | solution.py:22
  58.2 0.9 copy.50
  59.2 0.3 broadcast_in_dim.39
  59.5 0.7 pad_add_fusion
  60.2 1.7 %copy_bitcast_fusion = (bf16[6,128,2,32]{1,3,2,0:T(8,128)(2,1)}, bf16[6,128,2,32]{1,3,2,0:T(8,128)(2,1)}) fusion(bf16[768,2,32]{0,2,1:T(8,128)(2,1)} %copy-done.2, bf16[768,2,32]{0,2,1:T(8,128)(2,1)} %copy-done.3), kind=kLoop, calls=%fused_computation.46 | loop fusion | bytes 393216 | tf_op jit(solution)/shard_map/concatenate | solution.py:22
  61.9 1.6 %gather_fusion.3 = bf16[24,64,128]{2,1,0:T(8,128)(2,1)S(1)} fusion(bf16[24,64,128]{2,1,0:T(8,128)(2,1)} %bitcast.14, s32[1024]{0:T(1024)S(1)} %pad_clamp_fusion), kind=kCustom, calls=%fused_computation.3 | custom fusion | bytes 786528 | tf_op jit(solution)/shard_map/gather | solution.py:95
  63.5 1.2 %reshape.208 = bf16[6,256,2,64]{3,2,1,0:T(2,128)(2,1)} reshape(bf16[24,64,128]{2,1,0:T(8,128)(2,1)S(1)} %gather_fusion.3) | data formatting | bytes 786432 | tf_op jit(solution)/shard_map/reshape | solution.py:98
  64.8 2.9 %copy.56 = bf16[6,256,2,64]{1,3,2,0:T(8,128)(2,1)} copy(bf16[6,256,2,64]{3,2,1,0:T(2,128)(2,1)} %reshape.208) | data formatting | bytes 786432 | tf_op jit(solution)/shard_map/reshape | solution.py:98
  67.6 1.6 %gather_fusion.1 = bf16[24,64,128]{2,1,0:T(8,128)(2,1)S(1)} fusion(bf16[24,64,128]{2,1,0:T(8,128)(2,1)} %bitcast.4, s32[1024]{0:T(1024)S(1)} %pad_clamp_fusion), kind=kCustom, calls=%fused_computation.1 | custom fusion | bytes 786528 | tf_op jit(solution)/shard_map/gather | solution.py:96
  69.2 1.2 %reshape.205 = bf16[6,256,2,64]{3,2,1,0:T(2,128)(2,1)} reshape(bf16[24,64,128]{2,1,0:T(8,128)(2,1)S(1)} %gather_fusion.1) | data formatting | bytes 786432 | tf_op jit(solution)/shard_map/reshape | solution.py:99
  70.5 2.2 %copy.49 = bf16[6,256,2,64]{1,3,2,0:T(8,128)(2,1)S(1)} copy(bf16[6,256,2,64]{3,2,1,0:T(2,128)(2,1)} %reshape.205) | data formatting | bytes 786432 | tf_op jit(solution)/shard_map/reshape | solution.py:99
  72.7 8.9 %fusion.38 = (f32[6,2,4,128]{3,2,1,0:T(4,128)}, f32[6,2,4,128,384]{3,4,2,1,0:T(8,128)}) fusion(pred[6,128,384]{1,2,0:T(8,128)(4,1)} %pad_add_fusion, bf16[6,128,2,4,32]{1,4,3,2,0:T(8,128)(2,1)} %copy.59, bf16[6,128,2,4,32]{1,4,3,2,0:T(8,128)(2,1)} %copy.58, bf16[6,128,2,32]{1,3,2,0:T(8,128)(2,1)} %get-tuple-element.15, ...), kind=kOutput, calls=%fused_computation.74 | convolution fusion | flops 314769792 | bytes 11132928 | tf_op jit(solution)/shard_map/sub | solution.py:122
  81.5 4.8 %fusion.19 = bf16[6,128,2,4,64]{1,4,3,2,0:T(8,128)(2,1)S(1)} fusion(f32[6,2,4,128,384]{3,4,2,1,0:T(8,128)} %get-tuple-element.14, f32[6,2,4,128]{3,2,1,0:T(4,128)} %get-tuple-element.13, bf16[6,128,2,64]{1,3,2,0:T(8,128)(2,1)} %copy.50, bf16[6,256,2,64]{1,3,2,0:T(8,128)(2,1)S(1)} %copy.49), kind=kOutput, calls=%fused_computation.28 | convolution fusion | flops 308281344 | bytes 10838016 | tf_op jit(solution)/shard_map/bngqk,bknd->bqngd/dot_general | solution.py:125
  86.3 0.6 copy.61
  86.9 3.5 %convolution_convert_fusion = bf16[768,2048]{1,0:T(8,128)(2,1)} fusion(bf16[512,2048]{1,0:T(8,128)(2,1)S(1)} %copy-done.7, bf16[64,8,6,128]{3,2,1,0:T(8,128)(2,1)S(1)} %bitcast.96), kind=kOutput, calls=%fused_computation.16 | convolution fusion | flops 1612185600 | bytes 6029312 | tf_op jit(solution)/shard_map/dot_general | solution.py:129
  90.4 12.6 %reduce-scatter.2.cloned.1.call-done = bf16[768,1024]{1,0:T(8,128)(2,1)} async-done(((bf16[768,2048]{1,0:T(8,128)(2,1)}), bf16[768,1024]{1,0:T(8,128)(2,1)}) %reduce-scatter.2.cloned.1.call-update) | async-done | bytes 1572880 | tf_op jit(solution)/shard_map/reduce_scatter | solution.py:130
  103.0 1.8 %fusion.8 = f32[768]{0:T(1024)S(1)} fusion(bf16[768,1024]{1,0:T(8,128)(2,1)} %reduce-scatter.2.cloned.1.call-done), kind=kLoop, calls=%fused_computation.17 | loop fusion | flops 2358528 | bytes 1575936 | tf_op jit(solution)/shard_map/reduce_sum | solution.py:133
  104.8 2.5 %psum.7 = f32[768]{0:T(1024)S(1)} all-reduce(f32[768]{0:T(1024)S(1)} %fusion.8), channel_id=1, replica_groups=mesh['dp'=4,'kv'=4,'tp'=2] {'tp'}, use_global_device_ids=true, to_apply=%region_7.8 | all-reduce | flops 768 | bytes 6144 | tf_op jit(solution)/shard_map/psum | solution.py:133
  107.3 3.0 %fusion.17 = bf16[1,768,1024]{2,1,0:T(8,128)(2,1)} fusion(bf16[768,1024]{1,0:T(8,128)(2,1)} %reduce-scatter.2.cloned.1.call-done, f32[1024]{0:T(1024)S(1)} %copy-done.5, f32[768]{0:T(1024)S(1)} %add_rsqrt_fusion), kind=kLoop, calls=%fused_computation.26 | loop fusion | flops 3145728 | bytes 3152896 | tf_op jit(solution)/shard_map/broadcast_in_dim | solution.py:136
  (44 shorter events, 1.3 us)
Async XLA Ops:
  6.5 3.4 %copy-start = (bf16[1,768,2048]{2,1,0:T(8,128)(2,1)S(1)}, bf16[1,768,2048]{2,1,0:T(8,128)(2,1)}, u32[]{:S(2)}) copy-start(bf16[1,768,2048]{2,1,0:T(8,128)(2,1)} %param.8) | copy-start | bytes 9437188
  9.9 5.3 %copy-start.4 = (s32[1,24,4]{1,2,0:T(4,128)S(1)}, s32[1,24,4]{1,2,0:T(4,128)}, u32[]{:S(2)}) copy-start(s32[1,24,4]{1,2,0:T(4,128)} %param.14) | copy-start | bytes 1156
  12.2 0.6 copy-start.2
  12.2 0.7 copy-start.3
  20.7 22.3 %all-to-all-start.1 = ((bf16[4,6,64,128]{3,2,1,0:T(8,128)(2,1)}), bf16[4,6,64,128]{3,2,1,0:T(8,128)(2,1)}, u32[]{:S(2)}, u32[]{:S(2)}) async-start(bf16[4,6,64,128]{3,2,1,0:T(8,128)(2,1)} %bitcast.95), calls=%async_computation.1 | async-start | bytes 786432 | tf_op jit(solution)/shard_map/all_to_all | solution.py:91
  32.9 4.6 %copy-start.8 = (bf16[2048,128]{1,0:T(8,128)(2,1)S(1)}, bf16[2048,128]{1,0:T(8,128)(2,1)}, u32[]{:S(2)}) copy-start(bf16[2048,128]{1,0:T(8,128)(2,1)} %param.11) | copy-start | bytes 1572868
  40.6 9.2 %copy-start.6 = (pred[6,4]{0,1:T(4,128)(4,1)S(1)}, pred[6,4]{0,1:T(4,128)(4,1)}, u32[]{:S(2)}) copy-start(pred[6,4]{0,1:T(4,128)(4,1)} %fusion.43) | copy-start | bytes 76
  43.0 24.6 %all-to-all-start = ((bf16[4,6,64,128]{3,2,1,0:T(8,128)(2,1)}), bf16[4,6,64,128]{3,2,1,0:T(8,128)(2,1)}, u32[]{:S(2)}, u32[]{:S(2)}) async-start(bf16[4,6,64,128]{3,2,1,0:T(8,128)(2,1)} %bitcast.94), calls=%async_computation | async-start | bytes 786432 | tf_op jit(solution)/shard_map/all_to_all | solution.py:92
  48.1 54.9 %reduce-scatter.2.cloned.1.call-start = ((), (), s32[]{:S(2)}) async-start(), calls=%async_computation.3 | async-start | bytes 4718592 | tf_op jit(solution)/shard_map/reduce_scatter | solution.py:130
  49.7 8.5 %copy-start.1 = (bf16[6,128,2,64]{3,2,1,0:T(2,128)(2,1)S(1)}, bf16[6,128,2,64]{3,2,1,0:T(2,128)(2,1)}, u32[]{:S(2)}) copy-start(bf16[6,128,2,64]{3,2,1,0:T(2,128)(2,1)} %reshape.247) | copy-start | bytes 589828
  81.5 5.4 %copy-start.7 = (bf16[512,2048]{1,0:T(8,128)(2,1)S(1)}, bf16[512,2048]{1,0:T(8,128)(2,1)}, u32[]{:S(2)}) copy-start(bf16[512,2048]{1,0:T(8,128)(2,1)} %param.12) | copy-start | bytes 6291460
  90.4 16.9 %copy-start.5 = (f32[1024]{0:T(1024)S(1)}, f32[1024]{0:T(1024)}, u32[]{:S(2)}) copy-start(f32[1024]{0:T(1024)} %param.13) | copy-start | bytes 12292
Sparse Core Ops, SparseCore 0:
  90.5 12.3 reduce-scatter.1
where the time goes:
time: 118 us; the launch traced here: 117 us
  local copies, waits for them, and re-layouts  37.9 us (32%)
  matrix products  25 us (21%)
  other arithmetic  14.1 us (12%)
  between operations  13.6 us (12%)
  waiting for transfers between devices  12.6 us (11%)
  starting transfers between devices  11.4 us (10%)
  blocking collectives  2.47 us (2%)
    reduce_scatter x1, waiting for transfers between devices, body(): lax.psum_scatter(terms.astype(jnp.bfloat16), 'tp', scatter_dimension=1, t...  12.6 us
    concatenate x6, local copies, waits for them, and re-layouts, rotate(): jnp.concatenate([first_half * cosine - second_half * sine_part, second_ha...  11 us
    sub x1, matrix products, body(): weights = jnp.exp(scores - row_max)  8.85 us
    unnamed x22, local copies, waits for them, and re-layouts  7.87 us
    all_to_all x1, starting transfers between devices, body(): lax.all_to_all(send_keys, 'kv', split_axis=0, concat_axis=0, tiled=True)  6.35 us
    all_to_all x1, starting transfers between devices, body(): lax.all_to_all(send_values, 'kv', split_axis=0, concat_axis=0, tiled=True)  5.1 us
    dot_general x1, matrix products, body(): jnp.einsum('bngqk,bknd->bqngd', weights, all_values, preferred_element_ty...  4.79 us
    dot_general x1, matrix products, body(): jnp.dot(row_data, query_weight, preferred_element_type=jnp.float32)  4.62 us
  transfers between devices with their start and end apart: 3, of which 1 were waited for; matrix products, arithmetic and copies ran while one was open for 30% of the time, Pallas kernels for 0%

commit v1 on v0

--- a/solution.py
+++ b/solution.py
@@ -1,3 +1,4 @@
+import functools
 import jax
 import jax.numpy as jnp
 from jax import lax
@@ -9,6 +10,27 @@
 KEY_BLOCK = 64
 rope_base = 10000.0
 norm_eps = 1e-06
+
+
+def map_page_up(x0, along_dim, d_out):
+    left_arr, step_out = (lax.axis_size("kv"), lax.axis_index("kv"))
+    block_next = x0.shape[along_dim] // left_arr
+    piece_now = list(x0.shape)
+    piece_now[along_dim] = block_next
+    y_new = piece_now[d_out]
+    piece_now[d_out] = y_new * left_arr
+    w2 = jnp.zeros(piece_now, x0.dtype)
+    for ii in range(left_arr):
+        z2 = lax.dynamic_slice_in_dim(x0, (step_out ^ ii) * block_next, block_next, axis=along_dim)
+        if ii:
+            z2 = lax.ppermute(
+                z2, axis_name="kv", perm=[(dev_j, dev_j ^ ii) for dev_j in range(left_arr)]
+            )
+        w2 = lax.dynamic_update_slice_in_dim(w2, z2, (step_out ^ ii) * y_new, axis=d_out)
+    return w2
+
+
+chains_name = functools.partial(map_page_up, along_dim=0, d_out=0)
 
 
 def rotate(head_rows, positions):
@@ -88,7 +110,7 @@
     send_keys = key_blocks[wanted]
     send_values = value_blocks[wanted]
     got_keys, got_values = (
-        lax.all_to_all(send_keys, "kv", split_axis=0, concat_axis=0, tiled=True),
+        chains_name(send_keys),
         lax.all_to_all(send_values, "kv", split_axis=0, concat_axis=0, tiled=True),
     )
     slot_index = jnp.where(mine_valid, mine_owner * qblocks + rank_within(mine_owner), 0)

time: 118 us -> 125 us (1.059)
  local copies, waits for them, and re-layouts: 37.9 us -> 46.4 us
    all_to_all x1 -> x0, starting transfers between devices: 6.35 us -> none  [body(): lax.all_to_all(send_keys, 'kv', split_axis=0, concat_axis=0, tiled=True)]
    ppermute x0 -> x3, starting transfers between devices: none -> 5.82 us  [map_page_up(): lax.ppermute(z2, axis_name='kv', perm=[(dev_j, dev_j ^ ii) for dev_j in r...]
    dynamic_update_slice x0 -> x3, local copies, waits for them, and re-layouts: none -> 4.61 us  [map_page_up(): lax.dynamic_update_slice_in_dim(w2, z2, (step_out ^ ii) * y_new, axis=d_out)]
    concatenate x6, local copies, waits for them, and re-layouts: 11 us -> 9.04 us  [rotate(): jnp.concatenate([first_half * cosine - second_half * sine_part, second_ha...]
    dynamic_slice x0 -> x1, local copies, waits for them, and re-layouts: none -> 1.77 us  [map_page_up(): lax.dynamic_slice_in_dim(x0, (step_out ^ ii) * block_next, block_next, ax...]
    another operation x2, other arithmetic: 2.51 us -> 1.01 us
    broadcast_in_dim x2, local copies, waits for them, and re-layouts: 0.36 us -> 1.63 us  [body(): jnp.broadcast_to(key_valid[:, None, :], (qblocks, QUERY_BLOCK, chosen_cou...]
    unnamed x22 -> x24, local copies, waits for them, and re-layouts: 7.87 us -> 7.21 us
  transfers between devices with their start and end apart: 3 -> 5, of which waited for: 1 -> 1; matrix products, arithmetic and copies ran while one was open for 30% -> 41% of each run, Pallas kernels for 0% -> 0%
where the time goes in v1:
time: 125 us; the launch traced here: 124 us
  local copies, waits for them, and re-layouts  46.4 us (37%)
  matrix products  24.7 us (20%)
  between operations  13.6 us (11%)
  other arithmetic  13.2 us (11%)
  waiting for transfers between devices  12.6 us (10%)
  starting transfers between devices  10.7 us (9%)
  blocking collectives  2.48 us (2%)
    reduce_scatter x1, waiting for transfers between devices, body(): lax.psum_scatter(terms.astype(jnp.bfloat16), 'tp', scatter_dimension=1, t...  12.6 us
    concatenate x6, local copies, waits for them, and re-layouts, rotate(): jnp.concatenate([first_half * cosine - second_half * sine_part, second_ha...  9.04 us
    sub x1, matrix products, body(): weights = jnp.exp(scores - row_max)  8.7 us
    unnamed x24, local copies, waits for them, and re-layouts  7.21 us
    ppermute x3, starting transfers between devices, map_page_up(): lax.ppermute(z2, axis_name='kv', perm=[(dev_j, dev_j ^ ii) for dev_j in r...  5.82 us
    all_to_all x1, starting transfers between devices, body(): lax.all_to_all(send_values, 'kv', split_axis=0, concat_axis=0, tiled=True)  4.91 us
    dot_general x1, matrix products, body(): jnp.einsum('bngqk,bknd->bqngd', weights, all_values, preferred_element_ty...  4.8 us
    dynamic_update_slice x3, local copies, waits for them, and re-layouts, map_page_up(): lax.dynamic_update_slice_in_dim(w2, z2, (step_out ^ ii) * y_new, axis=d_out)  4.61 us
  transfers between devices with their start and end apart: 5, of which 1 were waited for; matrix products, arithmetic and copies ran while one was open for 41% of the time, Pallas kernels for 0%

profile of v1, /device:TPU:0, one launch (start us, length us, event | category | flops | bytes accessed | tf_op | source)
XLA Modules:
  0.0 123.7 jit_solution(3685920975023883176)
XLA Ops:
  7.1 2.3 %copy.52 = bf16[2048,128]{0,1:T(8,128)(2,1)} copy(bf16[2048,128]{1,0:T(8,128)(2,1)} %param.10) | data formatting | bytes 1048576 | tf_op args[2]
  9.9 2.3 %fusion.13 = f32[768,2,64]{0,2,1:T(8,128)S(1)} fusion(bf16[2,64,2048]{2,1,0:T(8,128)(2,1)} %bitcast.98, bf16[1,768,2048]{2,1,0:T(8,128)(2,1)S(1)} %copy-done), kind=kOutput, calls=%fused_computation.22 | convolution fusion | flops 402653184 | bytes 4063232 | tf_op jit(solution)/shard_map/dot_general | solution.py:80
  12.3 1.1 copy.53
  13.4 1.2 convert_element_type.47
  15.4 1.5 %convert_reduce_fusion = s32[4,24]{1,0:T(4,128)} fusion(s32[4,24]{1,0:T(4,128)S(1)} %reshape_squeeze.3, pred[24,24]{1,0:T(8,128)(4,1)} %iota_compare_fusion.2), kind=kLoop, calls=%fused_computation.50 | loop fusion | flops 9120 | bytes 1344 | tf_op jit(solution)/shard_map/vmap()/reduce_sum | solution.py:57
  16.9 0.8 copy.43
  17.7 0.9 select_reduce_fusion
  18.8 1.4 %gather_fusion.2 = bf16[24,64,128]{2,1,0:T(8,128)(2,1)} fusion(bf16[12,64,128]{2,1,0:T(8,128)(2,1)S(1)} %convert_element_type.47, s32[1024]{0:T(1024)S(1)} %pad_clamp_fusion.1), kind=kCustom, calls=%fused_computation.2 | custom fusion | bytes 786528 | tf_op jit(solution)/shard_map/gather | solution.py:110
  20.2 1.8 %constant_dynamic-slice_fusion.3 = (bf16[1,6,64,128]{3,2,1,0:T(8,128)(2,1)}, bf16[1,6,64,128]{3,2,1,0:T(8,128)(2,1)}, bf16[1,6,64,128]{3,2,1,0:T(8,128)(2,1)}, bf16[4,6,64,128]{3,2,1,0:T(8,128)(2,1)S(1)}) fusion(bf16[4,6,64,128]{3,2,1,0:T(8,128)(2,1)} %bitcast.95, s32[]{:T(128)S(6)} %select_n.68, s32[]{:T(128)S(6)} %select_n.67, s32[]{:T(128)S(6)} %select_n.66, ...), kind=kLoop, calls=%fused_computation.68 | loop fusion | bytes 786448 | tf_op jit(solution)/shard_map/dynamic_slice | solution.py:24
  22.0 3.1 %collective-permute-start = (bf16[1,6,64,128]{3,2,1,0:T(8,128)(2,1)}, bf16[1,6,64,128]{3,2,1,0:T(8,128)(2,1)}, u32[]{:S(2)}, u32[]{:S(2)}) collective-permute-start(bf16[1,6,64,128]{3,2,1,0:T(8,128)(2,1)} %get-tuple-element.13), channel_id=1, source_target_pairs={{0,2},{2,0},{4,6},{6,4},{1,3},{3,1},{5,7},{7,5},{8,10},{10,8},{12,... | collective-permute-start | bytes 294920 | tf_op jit(solution)/shard_map/ppermute | solution.py:26
  25.0 2.6 %collective-permute-start.1 = (bf16[1,6,64,128]{3,2,1,0:T(8,128)(2,1)}, bf16[1,6,64,128]{3,2,1,0:T(8,128)(2,1)}, u32[]{:S(2)}, u32[]{:S(2)}) collective-permute-start(bf16[1,6,64,128]{3,2,1,0:T(8,128)(2,1)} %get-tuple-element.12), channel_id=1, source_target_pairs={{0,4},{2,6},{4,0},{6,2},{1,5},{3,7},{5,1},{7,3},{8,12},{10,14},{12... | collective-permute-start | bytes 294920 | tf_op jit(solution)/shard_map/ppermute | solution.py:26
  27.8 2.0 %fusion.20 = bf16[768,128]{1,0:T(8,128)(2,1)S(1)} fusion(bf16[2048,128]{1,0:T(8,128)(2,1)} %param.11, bf16[1,768,2048]{2,1,0:T(8,128)(2,1)S(1)} %copy-done), kind=kOutput, calls=%fused_computation.30 | convolution fusion | flops 402751488 | bytes 3866624 | tf_op jit(solution)/shard_map/dot_general | solution.py:88
  29.8 1.4 %gather_fusion = bf16[24,64,128]{2,1,0:T(8,128)(2,1)} fusion(bf16[12,64,128]{2,1,0:T(8,128)(2,1)S(1)} %bitcast.93, s32[1024]{0:T(1024)S(1)} %pad_clamp_fusion.1), kind=kCustom, calls=%fused_computation | custom fusion | bytes 786528 | tf_op jit(solution)/shard_map/gather | solution.py:111
  31.2 4.9 %all-to-all-start = ((bf16[4,6,64,128]{3,2,1,0:T(8,128)(2,1)}), bf16[4,6,64,128]{3,2,1,0:T(8,128)(2,1)}, u32[]{:S(2)}, u32[]{:S(2)}) async-start(bf16[4,6,64,128]{3,2,1,0:T(8,128)(2,1)} %bitcast.94), calls=%async_computation | async-start | bytes 786432 | tf_op jit(solution)/shard_map/all_to_all | solution.py:114
  38.0 0.7 copy_bitcast_fusion
  38.8 0.9 reshape.247
  39.7 0.8 eq.59
  40.5 0.8 convert_reduce_fusion.1
  41.3 0.8 copy.45
  42.6 0.8 copy.46
  44.2 0.7 broadcast_in_dim.40
  44.8 4.0 %copy.57 = bf16[2048,512]{0,1:T(8,128)(2,1)} copy(bf16[2048,512]{1,0:T(8,128)(2,1)} %param.9) | data formatting | bytes 4194304 | tf_op args[1]
  48.8 3.4 %fusion.11 = f32[768,8,64]{0,2,1:T(8,128)S(1)} fusion(bf16[8,64,2048]{2,1,0:T(8,128)(2,1)} %bitcast.92, bf16[1,768,2048]{2,1,0:T(8,128)(2,1)S(1)} %copy-done), kind=kOutput, calls=%fused_computation.20 | convolution fusion | flops 1610612736 | bytes 6815744 | tf_op jit(solution)/shard_map/dot_general | solution.py:73
  52.3 1.0 subtract_convert_fusion
  53.3 2.2 %concatenate.37 = bf16[6,128,2,4,32]{1,0,4,3,2:T(8,128)(2,1)} reshape(bf16[768,8,32]{0,2,1:T(8,128)(2,1)} %get-tuple-element.7) | data formatting | bytes 786432 | tf_op jit(solution)/shard_map/concatenate | solution.py:44
  55.5 1.9 %copy.58 = bf16[6,128,2,4,32]{1,4,3,2,0:T(8,128)(2,1)} copy(bf16[6,128,2,4,32]{1,0,4,3,2:T(8,128)(2,1)} %concatenate.37) | data formatting | bytes 786432 | tf_op jit(solution)/shard_map/concatenate | solution.py:44
  57.4 1.2 %concatenate.38 = bf16[6,128,2,4,32]{1,0,4,3,2:T(8,128)(2,1)} reshape(bf16[768,8,32]{0,2,1:T(8,128)(2,1)S(1)} %get-tuple-element.8) | data formatting | bytes 786432 | tf_op jit(solution)/shard_map/concatenate | solution.py:44
  58.7 1.9 %copy.59 = bf16[6,128,2,4,32]{1,4,3,2,0:T(8,128)(2,1)} copy(bf16[6,128,2,4,32]{1,0,4,3,2:T(8,128)(2,1)} %concatenate.38) | data formatting | bytes 786432 | tf_op jit(solution)/shard_map/concatenate | solution.py:44
  60.5 1.8 %copy.50 = bf16[6,128,2,64]{1,3,2,0:T(8,128)(2,1)} copy(bf16[6,128,2,64]{3,2,1,0:T(2,128)(2,1)} %reshape.247) | data formatting | bytes 393216 | tf_op jit(solution)/shard_map/reshape | solution.py:126
  62.3 0.9 broadcast_in_dim.41
  63.3 0.7 pad_add_fusion
  64.1 0.7 fusion.29
  64.8 1.5 %constant_dynamic-update-slice_fusion.1 = bf16[4,6,64,128]{3,2,1,0:T(8,128)(2,1)} fusion(bf16[4,6,64,128]{3,2,1,0:T(8,128)(2,1)} %copy-done.1, bf16[1,6,64,128]{3,2,1,0:T(8,128)(2,1)} %collective-permute-done, s32[]{:T(128)S(6)} %select_n.66), kind=kLoop, calls=%fused_computation.64 | loop fusion | bytes 196612 | tf_op jit(solution)/shard_map/dynamic_update_slice | solution.py:29
  66.3 1.5 %constant_dynamic-update-slice_fusion = bf16[4,6,64,128]{3,2,1,0:T(8,128)(2,1)} fusion(bf16[4,6,64,128]{3,2,1,0:T(8,128)(2,1)} %constant_dynamic-update-slice_fusion.1, bf16[1,6,64,128]{3,2,1,0:T(8,128)(2,1)} %collective-permute-done.1, s32[]{:T(128)S(6)} %select_n.67), kind=kLoop, calls=%fused_computation.62 | loop fusion | bytes 196612 | tf_op jit(solution)/shard_map/dynamic_update_slice | solution.py:29
  67.9 1.5 %constant_dynamic-update-slice_fusion.2 = bf16[4,6,64,128]{3,2,1,0:T(8,128)(2,1)} fusion(bf16[4,6,64,128]{3,2,1,0:T(8,128)(2,1)} %constant_dynamic-update-slice_fusion, bf16[1,6,64,128]{3,2,1,0:T(8,128)(2,1)} %collective-permute-done.2, s32[]{:T(128)S(6)} %select_n.68), kind=kLoop, calls=%fused_computation.66 | loop fusion | bytes 196612 | tf_op jit(solution)/shard_map/dynamic_update_slice | solution.py:29
  69.4 1.6 %gather_fusion.3 = bf16[24,64,128]{2,1,0:T(8,128)(2,1)S(1)} fusion(bf16[24,64,128]{2,1,0:T(8,128)(2,1)} %bitcast.96, s32[1024]{0:T(1024)S(1)} %pad_clamp_fusion), kind=kCustom, calls=%fused_computation.3 | custom fusion | bytes 786528 | tf_op jit(solution)/shard_map/gather | solution.py:117
  71.0 1.2 reshape.208
  72.2 2.2 %copy.56 = bf16[6,256,2,64]{1,3,2,0:T(8,128)(2,1)S(1)} copy(bf16[6,256,2,64]{3,2,1,0:T(2,128)(2,1)} %reshape.208) | data formatting | bytes 786432 | tf_op jit(solution)/shard_map/reshape | solution.py:120
  74.4 8.7 %fusion.38 = (f32[6,2,4,128]{3,2,1,0:T(4,128)}, f32[6,2,4,128,384]{3,4,2,1,0:T(8,128)}) fusion(pred[6,128,384]{1,2,0:T(8,128)(4,1)} %pad_add_fusion, bf16[6,128,2,4,32]{1,4,3,2,0:T(8,128)(2,1)} %copy.59, bf16[6,128,2,4,32]{1,4,3,2,0:T(8,128)(2,1)} %copy.58, bf16[6,128,2,32]{1,3,2,0:T(8,128)(2,1)} %get-tuple-element.19, ...), kind=kOutput, calls=%fused_computation.81 | convolution fusion | flops 314769792 | bytes 11132928 | tf_op jit(solution)/shard_map/sub | solution.py:144
  83.1 1.6 %gather_fusion.1 = bf16[24,64,128]{2,1,0:T(8,128)(2,1)S(1)} fusion(bf16[24,64,128]{2,1,0:T(8,128)(2,1)} %bitcast.4, s32[1024]{0:T(1024)S(1)} %pad_clamp_fusion), kind=kCustom, calls=%fused_computation.1 | custom fusion | bytes 786528 | tf_op jit(solution)/shard_map/gather | solution.py:118
  84.8 1.2 reshape.205
  86.0 2.2 %copy.49 = bf16[6,256,2,64]{1,3,2,0:T(8,128)(2,1)S(1)} copy(bf16[6,256,2,64]{3,2,1,0:T(2,128)(2,1)} %reshape.205) | data formatting | bytes 786432 | tf_op jit(solution)/shard_map/reshape | solution.py:121
  88.2 4.8 %fusion.19 = bf16[6,128,2,4,64]{1,4,3,2,0:T(8,128)(2,1)S(1)} fusion(f32[6,2,4,128,384]{3,4,2,1,0:T(8,128)} %get-tuple-element.18, f32[6,2,4,128]{3,2,1,0:T(4,128)} %get-tuple-element.17, bf16[6,128,2,64]{1,3,2,0:T(8,128)(2,1)} %copy.50, bf16[6,256,2,64]{1,3,2,0:T(8,128)(2,1)S(1)} %copy.49), kind=kOutput, calls=%fused_computation.28 | convolution fusion | flops 308281344 | bytes 10838016 | tf_op jit(solution)/shard_map/bngqk,bknd->bqngd/dot_general | solution.py:147
  93.5 3.5 %convolution_convert_fusion = bf16[768,2048]{1,0:T(8,128)(2,1)} fusion(bf16[512,2048]{1,0:T(8,128)(2,1)S(1)} %copy-done.9, bf16[64,8,6,128]{3,2,1,0:T(8,128)(2,1)S(1)} %bitcast.97), kind=kOutput, calls=%fused_computation.16 | convolution fusion | flops 1612185600 | bytes 6029312 | tf_op jit(solution)/shard_map/dot_general | solution.py:151
  97.1 12.6 %reduce-scatter.2.cloned.1.call-done = bf16[768,1024]{1,0:T(8,128)(2,1)} async-done(((bf16[768,2048]{1,0:T(8,128)(2,1)}), bf16[768,1024]{1,0:T(8,128)(2,1)}) %reduce-scatter.2.cloned.1.call-update) | async-done | bytes 1572880 | tf_op jit(solution)/shard_map/reduce_scatter | solution.py:152
  109.6 1.8 %fusion.8 = f32[768]{0:T(1024)S(1)} fusion(bf16[768,1024]{1,0:T(8,128)(2,1)} %reduce-scatter.2.cloned.1.call-done), kind=kLoop, calls=%fused_computation.17 | loop fusion | flops 2358528 | bytes 1575936 | tf_op jit(solution)/shard_map/reduce_sum | solution.py:155
  111.4 2.5 %psum.7 = f32[768]{0:T(1024)S(1)} all-reduce(f32[768]{0:T(1024)S(1)} %fusion.8), channel_id=1, replica_groups=mesh['dp'=4,'kv'=4,'tp'=2] {'tp'}, use_global_device_ids=true, to_apply=%region_7.8 | all-reduce | flops 768 | bytes 6144 | tf_op jit(solution)/shard_map/psum | solution.py:155
  113.9 3.0 %fusion.17 = bf16[1,768,1024]{2,1,0:T(8,128)(2,1)} fusion(bf16[768,1024]{1,0:T(8,128)(2,1)} %reduce-scatter.2.cloned.1.call-done, f32[1024]{0:T(1024)S(1)} %copy-done.8, f32[768]{0:T(1024)S(1)} %add_rsqrt_fusion), kind=kLoop, calls=%fused_computation.26 | loop fusion | flops 3145728 | bytes 3152896 | tf_op jit(solution)/shard_map/broadcast_in_dim | solution.py:158
  (55 shorter events, 6.4 us)
Async XLA Ops:
  6.5 3.4 %copy-start = (bf16[1,768,2048]{2,1,0:T(8,128)(2,1)S(1)}, bf16[1,768,2048]{2,1,0:T(8,128)(2,1)}, u32[]{:S(2)}) copy-start(bf16[1,768,2048]{2,1,0:T(8,128)(2,1)} %param.8) | copy-start | bytes 9437188
  9.9 2.3 %copy-start.2 = (f32[768,32]{0,1:T(8,128)}, f32[768,32]{0,1:T(8,128)S(1)}, u32[]{:S(2)}) copy-start(f32[768,32]{0,1:T(8,128)S(1)} %get-tuple-element.15) | copy-start | bytes 294916
  9.9 2.3 %copy-start.4 = (f32[768,32]{0,1:T(8,128)}, f32[768,32]{0,1:T(8,128)S(1)}, u32[]{:S(2)}) copy-start(f32[768,32]{0,1:T(8,128)S(1)} %get-tuple-element.16) | copy-start | bytes 294916
  9.9 4.7 %copy-start.6 = (s32[1,24,4]{1,2,0:T(4,128)S(1)}, s32[1,24,4]{1,2,0:T(4,128)}, u32[]{:S(2)}) copy-start(s32[1,24,4]{1,2,0:T(4,128)} %param.14) | copy-start | bytes 1156
  22.0 5.6 %copy-start.1 = (bf16[4,6,64,128]{3,2,1,0:T(8,128)(2,1)}, bf16[4,6,64,128]{3,2,1,0:T(8,128)(2,1)S(1)}, u32[]{:S(2)}) copy-start(bf16[4,6,64,128]{3,2,1,0:T(8,128)(2,1)S(1)} %get-tuple-element.14) | copy-start | bytes 1179652
  22.0 42.8 %collective-permute-start = (bf16[1,6,64,128]{3,2,1,0:T(8,128)(2,1)}, bf16[1,6,64,128]{3,2,1,0:T(8,128)(2,1)}, u32[]{:S(2)}, u32[]{:S(2)}) collective-permute-start(bf16[1,6,64,128]{3,2,1,0:T(8,128)(2,1)} %get-tuple-element.13), channel_id=1, source_target_pairs={{0,2},{2,0},{4,6},{6,4},{1,3},{3,1},{5,7},{7,5},{8,10},{10,8},{12,... | collective-permute-start | bytes 294920 | tf_op jit(solution)/shard_map/ppermute | solution.py:26
  25.0 41.3 %collective-permute-start.1 = (bf16[1,6,64,128]{3,2,1,0:T(8,128)(2,1)}, bf16[1,6,64,128]{3,2,1,0:T(8,128)(2,1)}, u32[]{:S(2)}, u32[]{:S(2)}) collective-permute-start(bf16[1,6,64,128]{3,2,1,0:T(8,128)(2,1)} %get-tuple-element.12), channel_id=1, source_target_pairs={{0,4},{2,6},{4,0},{6,2},{1,5},{3,7},{5,1},{7,3},{8,12},{10,14},{12... | collective-permute-start | bytes 294920 | tf_op jit(solution)/shard_map/ppermute | solution.py:26
  27.6 8.5 %copy-start.7 = (s32[1,24,4]{1,2,0:T(4,128)S(1)}, s32[1,24,4]{1,2,0:T(4,128)}, u32[]{:S(2)}) copy-start(s32[1,24,4]{1,2,0:T(4,128)} %param.14) | copy-start | bytes 1156
  27.6 40.2 %collective-permute-start.2 = (bf16[1,6,64,128]{3,2,1,0:T(8,128)(2,1)}, bf16[1,6,64,128]{3,2,1,0:T(8,128)(2,1)}, u32[]{:S(2)}, u32[]{:S(2)}) collective-permute-start(bf16[1,6,64,128]{3,2,1,0:T(8,128)(2,1)} %get-tuple-element.11), channel_id=1, source_target_pairs={{0,6},{2,4},{4,2},{6,0},{1,7},{3,5},{5,3},{7,1},{8,14},{10,12},{12... | collective-permute-start | bytes 294920 | tf_op jit(solution)/shard_map/ppermute | solution.py:26
  31.2 51.9 %all-to-all-start = ((bf16[4,6,64,128]{3,2,1,0:T(8,128)(2,1)}), bf16[4,6,64,128]{3,2,1,0:T(8,128)(2,1)}, u32[]{:S(2)}, u32[]{:S(2)}) async-start(bf16[4,6,64,128]{3,2,1,0:T(8,128)(2,1)} %bitcast.94), calls=%async_computation | async-start | bytes 786432 | tf_op jit(solution)/shard_map/all_to_all | solution.py:114
  36.1 73.5 %reduce-scatter.2.cloned.1.call-start = ((), (), s32[]{:S(2)}) async-start(), calls=%async_computation.2 | async-start | bytes 4718592 | tf_op jit(solution)/shard_map/reduce_scatter | solution.py:152
  48.8 3.5 %copy-start.3 = (f32[768,32]{0,1:T(8,128)S(1)}, f32[768,32]{0,1:T(8,128)}, u32[]{:S(2)}) copy-start(f32[768,32]{0,1:T(8,128)} %copy-done.2) | copy-start | bytes 294916
  48.8 3.5 %copy-start.5 = (f32[768,32]{0,1:T(8,128)S(1)}, f32[768,32]{0,1:T(8,128)}, u32[]{:S(2)}) copy-start(f32[768,32]{0,1:T(8,128)} %copy-done.4) | copy-start | bytes 294916
  88.2 5.4 %copy-start.9 = (bf16[512,2048]{1,0:T(8,128)(2,1)S(1)}, bf16[512,2048]{1,0:T(8,128)(2,1)}, u32[]{:S(2)}) copy-start(bf16[512,2048]{1,0:T(8,128)(2,1)} %param.12) | copy-start | bytes 6291460
  97.0 16.9 %copy-start.8 = (f32[1024]{0:T(1024)S(1)}, f32[1024]{0:T(1024)}, u32[]{:S(2)}) copy-start(f32[1024]{0:T(1024)} %param.13) | copy-start | bytes 12292
Sparse Core Ops, SparseCore 0:
  97.2 12.3 reduce-scatter.1
